TPU v7x, 32 devices: a whole 2x2x4 slice. The times are simulated.
32 devices in a mesh: sp: 8 (over z, x), tp: 4 (over y, core).
Axes of the slice: x: 2, y: 2, z: 4, core: 2. Of those that a mesh axis runs over, the one named last changes fastest.
Arguments:
- tokens: bfloat16 [4096, 2048], P(('sp', 'tp')), may hold values from -6 to 6
- norm_gain: float32 [2048], replicated, may hold values from 0.1 to 1.9
- w_query: bfloat16 [2048, 1024], P(None, 'tp'), may hold values from -16 to 16
- w_key: bfloat16 [2048, 1024], P(None, 'tp'), may hold values from -16 to 16
- w_value: bfloat16 [2048, 1024], P(None, 'tp'), may hold values from -0.125 to 0.125
- conv_in: bfloat16 [2048, 2048], P(None, 'tp'), may hold values from -0.125 to 0.125
- conv_gate: bfloat16 [2048, 2048], P(None, 'tp'), may hold values from -0.125 to 0.125
- conv_taps: float32 [31, 2048], P(None, 'tp'), may hold values from -3.7 to 3.7
- conv_gain: float32 [2048], P('tp'), may hold values from 0.1 to 1.9
- cum_gate: float32 [16, 4096], P('tp'), may hold values from -514 to 0, as said below
- out_attn: bfloat16 [1024, 2048], P('tp'), may hold values from -0.75 to 0.75
- out_conv: bfloat16 [2048, 2048], P('tp'), may hold values from -0.125 to 0.125
Outputs:
- mixed: bfloat16 [4096, 2048], P(('sp', 'tp'))
- log_total: float32 [16, 4096], P('tp', 'sp')
Inputs may be any that keep to these rules, and one draw needn't show every extreme that they name: `cum_gate`: for each head the values never rise from one position to the next and are at most 0.
All inputs are finite; a program needn't handle non-finite values.
Results may differ from a plain program's by a relative error of at most 0.014.
Values may be sent and summed in bfloat16 or wider, within the bound.
A program may use at most 128 MiB of HBM per device.

v0:
```python
import jax
import jax.numpy as jnp
from jax import lax
from jax.sharding import PartitionSpec as P

HEAD = 64


def shifted(array, axis, by):
    length = lax.axis_size(axis)
    pairs = [(i, i + by) for i in range(length) if 0 <= i + by < length]
    return lax.ppermute(array, axis, pairs)


def per_device(
    tokens,
    norm_gain,
    w_query,
    w_key,
    w_value,
    conv_in,
    conv_gate,
    conv_taps,
    conv_gain,
    cum_gate,
    out_attn,
    out_conv,
):
    heads_here = w_query.shape[1] // HEAD
    width_att = w_query.shape[1]
    channels = conv_in.shape[1]
    kernel_len = conv_taps.shape[0]
    wide = lax.all_gather(tokens, "tp", axis=0, tiled=True).astype(jnp.float32)
    factor = lax.rsqrt(jnp.mean(wide * wide, axis=1, keepdims=True) + 1e-06)
    normed = (wide * factor * norm_gain[None, :]).astype(jnp.bfloat16)
    query = (jnp.dot(normed, w_query, preferred_element_type=jnp.float32) * HEAD ** (-0.5)).astype(
        jnp.bfloat16
    )
    keyed = jnp.dot(normed, w_key, preferred_element_type=jnp.float32).astype(jnp.bfloat16)
    valued = jnp.dot(normed, w_value, preferred_element_type=jnp.float32).astype(jnp.bfloat16)
    opened = jnp.dot(normed, conv_in, preferred_element_type=jnp.float32)
    gating = jnp.dot(normed, conv_gate, preferred_element_type=jnp.float32)
    gated_rows = (opened * jax.nn.sigmoid(gating)).astype(jnp.bfloat16)
    joined = jnp.concatenate([query, keyed, valued, gated_rows], axis=1)
    local_rows = joined.shape[0]
    own_index = lax.axis_index("sp")
    offset = own_index * local_rows
    query_rows = joined[:, :width_att]
    key_rows = joined[:, width_att : 2 * width_att]
    value_rows = joined[:, 2 * width_att : 3 * width_att]
    gated = joined[:, 3 * width_att :]
    group_list = (query_rows, offset)
    group_data = []
    group_rows, group_start = group_list
    count_rows = group_rows.shape[0]
    group_data.append(
        (
            group_rows.reshape(count_rows, heads_here, HEAD),
            lax.dynamic_slice_in_dim(cum_gate, group_start, count_rows, 1),
            group_start + jnp.arange(count_rows, dtype=jnp.int32),
            group_start + count_rows - 1,
        )
    )

    def absorb(carry_in, group, key_block, value_block, first_place):
        query_heads, cum_query, query_place, last_query = group
        row_best, row_total, row_accum = carry_in
        length_in = key_block.shape[0]
        key_heads = key_block.reshape(length_in, heads_here, HEAD)
        value_heads = value_block.reshape(length_in, heads_here, HEAD)
        cum_keys = lax.dynamic_slice_in_dim(cum_gate, first_place, length_in, 1)
        scores = jnp.einsum(
            "qhd,khd->hqk", query_heads, key_heads, preferred_element_type=jnp.float32
        )
        scores = scores + cum_query[:, :, None] - cum_keys[:, None, :]
        key_place = first_place + jnp.arange(length_in, dtype=jnp.int32)
        visible = jnp.logical_and(
            key_place[None, :] <= query_place[:, None], key_place[None, :] >= 0
        )[None]
        scores = jnp.where(visible, scores, -1e30)
        new_best = jnp.maximum(row_best, jnp.max(scores, axis=2))
        shrink = jnp.exp(row_best - new_best)
        weights = jnp.where(visible, jnp.exp(scores - new_best[:, :, None]), 0.0)
        row_total = shrink * row_total + jnp.sum(weights, axis=2)
        row_accum = shrink[:, :, None] * row_accum + jnp.einsum(
            "hqk,khd->hqd",
            weights.astype(jnp.bfloat16),
            value_heads,
            preferred_element_type=jnp.float32,
        )
        return (new_best, row_total, row_accum)

    initial = tuple(
        (
            (
                jnp.full((heads_here, group[0].shape[0]), -1e30, jnp.float32),
                jnp.zeros((heads_here, group[0].shape[0]), jnp.float32),
                jnp.zeros((heads_here, group[0].shape[0], HEAD), jnp.float32),
            )
            for group in group_data
        )
    )
    key_group = lax.all_gather(key_rows, "sp", axis=0, tiled=True)
    value_group = lax.all_gather(value_rows, "sp", axis=0, tiled=True)
    length_in = key_group.shape[0]
    turns = length_in // local_rows

    def advance(turn_index, carry_now):
        begin_row = turn_index * local_rows
        key_block = lax.dynamic_slice_in_dim(key_group, begin_row, local_rows, 0)
        value_block = lax.dynamic_slice_in_dim(value_group, begin_row, local_rows, 0)
        updated = []
        for group, inner_carry in zip(group_data, carry_now):
            wanted = jnp.logical_and(begin_row <= group[3], begin_row + local_rows > 0)

            def take_block(inner, group=group):
                return absorb(inner, group, key_block, value_block, begin_row)

            def skip_block(inner):
                return inner

            updated.append(lax.cond(wanted, take_block, skip_block, inner_carry))
        return tuple(updated)

    carry = lax.fori_loop(0, turns, advance, initial)
    attended_parts = []
    total_parts = []
    for row_best, row_total, row_accum in carry:
        count_rows = row_total.shape[1]
        attended_parts.append(
            (row_accum / row_total[:, :, None])
            .astype(jnp.bfloat16)
            .transpose(1, 0, 2)
            .reshape(count_rows, width_att)
        )
        total_parts.append(row_best + jnp.log(row_total))
    attended = attended_parts[0]
    log_total = total_parts[0]
    rim_rows = shifted(gated[local_rows - (kernel_len - 1) :], "sp", 1)
    padded = jnp.concatenate([rim_rows, gated], axis=0).astype(jnp.float32)
    convolved = jnp.zeros((local_rows, channels), jnp.float32)
    for tap_index in range(kernel_len):
        convolved = (
            convolved + conv_taps[tap_index][None, :] * padded[tap_index : tap_index + local_rows]
        )
    all_channels = channels * lax.axis_size("tp")
    channel_square = lax.psum(jnp.sum(convolved * convolved, axis=1), "tp") / all_channels
    conv_out = jax.nn.silu(
        convolved * lax.rsqrt(channel_square + 1e-06)[:, None] * conv_gain[None, :]
    ).astype(jnp.bfloat16)
    group_part = jnp.dot(attended, out_attn, preferred_element_type=jnp.float32)
    group_part = group_part + jnp.dot(conv_out, out_conv, preferred_element_type=jnp.float32)
    mixed = lax.psum_scatter(
        lax.optimization_barrier(group_part.astype(jnp.bfloat16))
        .astype(jnp.float32)
        .astype(jnp.bfloat16),
        "tp",
        scatter_dimension=0,
        tiled=True,
    )
    return (mixed, log_total)


def solution(mesh):
    in_specs = (
        P(("sp", "tp"), None),
        P(),
        P(None, "tp"),
        P(None, "tp"),
        P(None, "tp"),
        P(None, "tp"),
        P(None, "tp"),
        P(None, "tp"),
        P("tp"),
        P("tp", None),
        P("tp", None),
        P("tp", None),
    )
    out_specs = (P(("sp", "tp"), None), P("tp", "sp"))
    return jax.shard_map(
        per_device, mesh=mesh, in_specs=in_specs, out_specs=out_specs, check_vma=False
    )
```

profile of v0, /device:TPU:0, one launch (start us, length us, event | category | flops | bytes accessed | tf_op | source)
XLA Modules:
  0.0 236.0 jit_solution(1296425185891095124)
XLA Ops:
  8.0 26.9 %all-gather.4.cloned.1.call-done = bf16[512,2048]{1,0:T(8,128)(2,1)} async-done(((bf16[128,2048]{1,0:T(8,128)(2,1)}), bf16[512,2048]{1,0:T(8,128)(2,1)}) %all-gather.4.cloned.1.call-update) | async-done | bytes 2097168 | tf_op jit(solution)/shard_map/all_gather | solution.py:33
  34.9 2.1 fusion.13
  37.0 3.3 %convolution_convert_fusion.1 = bf16[512,256]{1,0:T(8,128)(2,1)} fusion(bf16[2048,256]{1,0:T(8,128)(2,1)} %param.19, bf16[512,2048]{1,0:T(8,128)(2,1)} %all-gather.4.cloned.1.call-done, f32[2048]{0:T(1024)} %param.17, f32[512]{0:T(512)S(1)} %add_rsqrt_fusion.1), kind=kOutput, calls=%fused_computation.35 | convolution fusion | flops 541196288 | bytes 3418112 | tf_op jit(solution)/shard_map/dot_general | solution.py:39
  40.4 3.0 %convolution_convert_fusion = bf16[512,256]{1,0:T(8,128)(2,1)} fusion(bf16[2048,256]{1,0:T(8,128)(2,1)S(1)} %copy-done.5, bf16[512,2048]{1,0:T(8,128)(2,1)} %all-gather.4.cloned.1.call-done, f32[2048]{0:T(1024)S(1)} %copy-done.7, f32[512]{0:T(512)S(1)} %add_rsqrt_fusion.1), kind=kOutput, calls=%fused_computation.34 | convolution fusion | flops 541196288 | bytes 3418112 | tf_op jit(solution)/shard_map/dot_general | solution.py:40
  44.3 3.8 %fusion.18 = f32[512,512]{1,0:T(8,128)S(1)} fusion(bf16[2048,512]{1,0:T(8,128)(2,1)} %param.22, bf16[512,2048]{1,0:T(8,128)(2,1)} %all-gather.4.cloned.1.call-done, f32[2048]{0:T(1024)S(1)} %copy-done.7, f32[512]{0:T(512)S(1)} %add_rsqrt_fusion.1), kind=kOutput, calls=%fused_computation.30 | convolution fusion | flops 1078722560 | bytes 5253120 | tf_op jit(solution)/shard_map/dot_general | solution.py:42
  48.2 1.3 fusion.19
  49.5 3.4 %collective-permute-start = (bf16[30,512]{1,0:T(8,128)(2,1)S(1)}, bf16[30,512]{1,0:T(8,128)(2,1)S(1)}, u32[]{:S(2)}, u32[]{:S(2)}) collective-permute-start(bf16[30,512]{1,0:T(8,128)(2,1)S(1)} %slice.252), channel_id=1, source_target_pairs={{0,4},{4,8},{8,12},{12,16},{16,20},{20,24},{24,28},{1,5},{5,9},{9,... | collective-permute-start | bytes 92168 | tf_op jit(solution)/shard_map/ppermute | solution.py:12
  52.9 1.0 fusion.20
  54.6 5.7 %multiply_reduce_fusion = (f32[512]{0:T(512)S(1)}, f32[512,512]{1,0:T(8,128)}) fusion(f32[542,512]{1,0:T(8,128)S(1)} %maximum_convert_fusion, f32[512]{0:T(512)S(1)} %bitcast.72, f32[512]{0:T(512)S(1)} %bitcast.73, f32[512]{0:T(512)S(1)} %bitcast.75, f32[512]{0:T(512)S(1)} %bitcast.76, f32[512]{0:T(512)S(1)} %bitcast.77, f32[512]{0:T(512)S(1)} %bitcast.78, ...), kind=kLoop, calls=%fused_computation.98 | loop fusion | flops 16514560 | bytes 33619968 | tf_op jit(solution)/shard_map/reduce_sum | solution.py:147
  60.3 6.1 %psum.7 = f32[512]{0:T(512)S(1)} all-reduce(f32[512]{0:T(512)S(1)} %get-tuple-element.390), channel_id=1, replica_groups=mesh['sp'=8,'tp'=4] {'tp'}, use_global_device_ids=true, to_apply=%region_8.9 | all-reduce | flops 512 | bytes 4096 | tf_op jit(solution)/shard_map/psum | solution.py:147
  66.4 23.3 %all-gather.6.cloned.1.call-done = bf16[4096,256]{1,0:T(8,128)(2,1)} async-done(((bf16[512,256]{1,0:T(8,128)(2,1)}), bf16[4096,256]{1,0:T(8,128)(2,1)}) %all-gather.6.cloned.1.call-update) | async-done | bytes 2097168 | tf_op jit(solution)/shard_map/all_gather | solution.py:103
  89.7 4.1 %copy.15 = bf16[4096,256]{0,1:T(8,128)(2,1)} copy(bf16[4096,256]{1,0:T(8,128)(2,1)} %all-gather.6.cloned.1.call-done) | data formatting | bytes 4194304
  93.8 45.7 %all-gather.8.cloned.1.call-done = bf16[4096,256]{1,0:T(8,128)(2,1)} async-done(((bf16[512,256]{1,0:T(8,128)(2,1)}), bf16[4096,256]{1,0:T(8,128)(2,1)}) %all-gather.8.cloned.1.call-update) | async-done | bytes 2097168 | tf_op jit(solution)/shard_map/all_gather | solution.py:104
  139.5 4.1 %copy.16 = bf16[4096,256]{0,1:T(8,128)(2,1)} copy(bf16[4096,256]{1,0:T(8,128)(2,1)} %all-gather.8.cloned.1.call-done) | data formatting | bytes 4194304
  143.7 6.8 %while.18 = (s32[]{:T(128)}, f32[4,512]{1,0:T(4,128)S(1)}, f32[4,512]{1,0:T(4,128)S(1)}, f32[4,512,64]{1,2,0:T(8,128)S(1)}, s32[]{:T(128)}, /*index=5*/bf16[4096...) while((s32[]{:T(128)}, f32[4,512]{1,0:T(4,128)S(1)}, ...), condition=%wide.region_6.7_spmd.clone, body=%wide.region_1.6_spmd.clone.sunk | while | flops 286005248 | bytes 16725373 | solution.py:125
  143.8 6.3 %conditional.3 = ((f32[4,512]{1,0:T(4,128)S(1)}, f32[4,512]{1,0:T(4,128)S(1)}, f32[4,512,64]{1,2,0:T(8,128)S(1)})) conditional(s32[]{:T(128)} %convert_element_type.89, (f32[4,512]{1,0:T(4,128)S(1)}, f32[4,512]{1,0:T(4,128)S(1)}, f32[4,512,64]{1,2,0:T(8,128)S(1)}) %tuple.88, (s32[]{:T(128)}, s32[]{:T(128)}, bf16[4096,256]{0,1:T(8,128)(2,1)}, ...), branch_computations={%region_2.0_spmd, %region_3.5_spmd} | conditional | flops 286005248 | bytes 16723030 | solution.py:122
  144.1 0.7 constant_dynamic-slice_fusion.1
  144.8 1.1 constant_dynamic-slice_fusion
  145.8 1.2 fusion.4
  147.0 1.4 fusion.3
  148.4 1.6 fusion.8
  150.6 2.0 fusion.63
  152.7 2.8 %add_convert_fusion = bf16[512,2048]{1,0:T(8,128)(2,1)} fusion(f32[512,2048]{1,0:T(8,128)S(1)} %fusion.63, bf16[512,2048]{1,0:T(8,128)(2,1)S(1)} %copy-done, f32[512,512]{1,0:T(8,128)S(1)} %copy-done.2, f32[512]{0:T(512)S(1)} %copy-done.8, f32[512]{0:T(512)S(1)} %add_rsqrt_fusion), kind=kOutput, calls=%fused_computation.25 | convolution fusion | flops 1077673984 | bytes 9441280 | tf_op jit(solution)/shard_map/dot_general | solution.py:152
  156.1 73.3 %reduce-scatter.2.cloned.1.call-done = bf16[128,2048]{1,0:T(8,128)(2,1)} async-done(((bf16[512,2048]{1,0:T(8,128)(2,1)}), bf16[128,2048]{1,0:T(8,128)(2,1)}) %reduce-scatter.2.cloned.1.call-update) | async-done | bytes 524304 | tf_op jit(solution)/shard_map/reduce_scatter | solution.py:153
  (60 shorter events, 3.6 us)
Async XLA Ops:
  7.2 145.5 %copy-start = (bf16[512,2048]{1,0:T(8,128)(2,1)S(1)}, bf16[512,2048]{1,0:T(8,128)(2,1)}, u32[]{:S(2)}) copy-start(bf16[512,2048]{1,0:T(8,128)(2,1)} %param.27) | copy-start | bytes 6291460
  7.2 27.7 %all-gather.4.cloned.1.call-start = ((), (), s32[]{:S(2)}) async-start(), calls=%async_computation.1 | async-start | bytes 2621440 | tf_op jit(solution)/shard_map/all_gather | solution.py:33
  7.9 32.5 %copy-start.5 = (bf16[2048,256]{1,0:T(8,128)(2,1)S(1)}, bf16[2048,256]{1,0:T(8,128)(2,1)}, u32[]{:S(2)}) copy-start(bf16[2048,256]{1,0:T(8,128)(2,1)} %param.20) | copy-start | bytes 3145732
  7.9 32.5 %copy-start.7 = (f32[2048]{0:T(1024)S(1)}, f32[2048]{0:T(1024)}, u32[]{:S(2)}) copy-start(f32[2048]{0:T(1024)} %param.17) | copy-start | bytes 24580
  7.9 81.8 %all-gather.6.cloned.1.call-start = ((), (), s32[]{:S(2)}) async-start(), calls=%async_computation.2 | async-start | bytes 2359296 | tf_op jit(solution)/shard_map/all_gather | solution.py:103
  40.3 3.9 %copy-start.3 = (f32[31,512]{1,0:T(8,128)S(1)}, f32[31,512]{1,0:T(8,128)}, u32[]{:S(2)}) copy-start(f32[31,512]{1,0:T(8,128)} %param.23) | copy-start | bytes 190468
  40.3 99.2 %all-gather.8.cloned.1.call-start = ((), (), s32[]{:S(2)}) async-start(), calls=%async_computation.3 | async-start | bytes 2359296 | tf_op jit(solution)/shard_map/all_gather | solution.py:104
  43.5 186.0 %reduce-scatter.2.cloned.1.call-start = ((), (), s32[]{:S(2)}) async-start(), calls=%async_computation.4 | async-start | bytes 2621440 | tf_op jit(solution)/shard_map/reduce_scatter | solution.py:153
  44.3 3.8 %copy-start.1 = (bf16[512,2048]{1,0:T(8,128)(2,1)S(1)}, bf16[512,2048]{1,0:T(8,128)(2,1)}, u32[]{:S(2)}) copy-start(bf16[512,2048]{1,0:T(8,128)(2,1)} %all-gather.4.cloned.1.call-done) | copy-start | bytes 6291460
  44.3 3.8 %copy-start.4 = (bf16[2048,512]{1,0:T(8,128)(2,1)S(1)}, bf16[2048,512]{1,0:T(8,128)(2,1)}, u32[]{:S(2)}) copy-start(bf16[2048,512]{1,0:T(8,128)(2,1)} %param.21) | copy-start | bytes 6291460
  48.1 4.7 %copy-start.6 = (bf16[2048,256]{1,0:T(8,128)(2,1)S(1)}, bf16[2048,256]{1,0:T(8,128)(2,1)}, u32[]{:S(2)}) copy-start(bf16[2048,256]{1,0:T(8,128)(2,1)} %param.18) | copy-start | bytes 3145732
  49.5 5.0 %collective-permute-start = (bf16[30,512]{1,0:T(8,128)(2,1)S(1)}, bf16[30,512]{1,0:T(8,128)(2,1)S(1)}, u32[]{:S(2)}, u32[]{:S(2)}) collective-permute-start(bf16[30,512]{1,0:T(8,128)(2,1)S(1)} %slice.252), channel_id=1, source_target_pairs={{0,4},{4,8},{8,12},{12,16},{16,20},{20,24},{24,28},{1,5},{5,9},{9,... | collective-permute-start | bytes 92168 | tf_op jit(solution)/shard_map/ppermute | solution.py:12
  150.5 2.1 copy-start.2
  150.5 2.1 copy-start.8
Sparse Core Ops, SparseCore 0:
  9.5 25.2 all-gather.3
  40.4 49.2 all-gather.5
  91.9 47.6 all-gather.7
  155.6 73.7 reduce-scatter.1
where the time goes:
time: 237 us; the launch traced here: 236 us
  waiting for transfers between devices  171 us (72%)
  matrix products  20.1 us (8%)
  between operations  14 us (6%)
  local copies, waits for them, and re-layouts  10.9 us (5%)
  other arithmetic  10.3 us (4%)
  blocking collectives  6.08 us (3%)
  starting transfers between devices  3.54 us (1%)
    reduce_scatter x1, waiting for transfers between devices, per_device(): lax.psum_scatter(lax.optimization_barrier(group_part.astype(jnp.bfloat16)...  73.3 us
    all_gather x1, waiting for transfers between devices, per_device(): value_group = lax.all_gather(value_rows, 'sp', axis=0, tiled=True)  45.7 us
    all_gather x1, waiting for transfers between devices, per_device(): wide = lax.all_gather(tokens, 'tp', axis=0, tiled=True).astype(jnp.float32)  26.9 us
    all_gather x1, waiting for transfers between devices, per_device(): key_group = lax.all_gather(key_rows, 'sp', axis=0, tiled=True)  23.3 us
    unnamed x20, local copies, waits for them, and re-layouts  8.28 us
    psum x1, blocking collectives, per_device(): lax.psum(jnp.sum(convolved * convolved, axis=1), 'tp') / all_channels  6.08 us
    reduce_sum x1, other arithmetic, per_device(): jnp.sum(convolved * convolved, axis=1)  5.69 us
  transfers between devices with their start and end apart: 5, of which 5 were waited for; matrix products, arithmetic and copies ran while one was open for 9% of the time, Pallas kernels for 0%

commit v1 on v0

--- a/solution.py
+++ b/solution.py
@@ -101,7 +101,12 @@
         )
     )
     key_group = lax.all_gather(key_rows, "sp", axis=0, tiled=True)
-    value_group = lax.all_gather(value_rows, "sp", axis=0, tiled=True)
+    ring = [value_rows]
+    for hop in range(7):
+        ring.append(lax.ppermute(ring[-1], "sp", [(dev, (dev + 1) % 8) for dev in range(8)]))
+    value_group = jnp.roll(
+        jnp.concatenate(ring[::-1], axis=0), (lax.axis_index("sp") + 1) * ring[0].shape[0], axis=0
+    )
     length_in = key_group.shape[0]
     turns = length_in // local_rows
 

time: 237 us -> 230 us (0.970)
  waiting for transfers between devices: 171 us -> 157 us
  local copies, waits for them, and re-layouts: 10.9 us -> 17.5 us
    ppermute x0 -> x7, waiting for transfers between devices: none -> 57.2 us  [per_device(): lax.ppermute(ring[-1], 'sp', [(dev, (dev + 1) % 8) for dev in range(8)])]
    all_gather x1 -> x0, waiting for transfers between devices: 45.7 us -> none  [per_device(): value_group = lax.all_gather(value_rows, 'sp', axis=0, tiled=True)]
    all_gather x1, waiting for transfers between devices: 23.3 us -> 0.01 us  [per_device(): key_group = lax.all_gather(key_rows, 'sp', axis=0, tiled=True)]
    unnamed x20 -> x39, local copies, waits for them, and re-layouts: 8.28 us -> 13.3 us
  transfers between devices with their start and end apart: 5 -> 11, of which waited for: 5 -> 9; matrix products, arithmetic and copies ran while one was open for 9% -> 12% of each run, Pallas kernels for 0% -> 0%
where the time goes in v1:
time: 230 us; the launch traced here: 229 us
  waiting for transfers between devices  157 us (68%)
  matrix products  20.4 us (9%)
  local copies, waits for them, and re-layouts  17.5 us (8%)
  between operations  14.1 us (6%)
  other arithmetic  10.2 us (4%)
  blocking collectives  6.22 us (3%)
  starting transfers between devices  2.94 us (1%)
    reduce_scatter x1, waiting for transfers between devices, per_device(): lax.psum_scatter(lax.optimization_barrier(group_part.astype(jnp.bfloat16)...  72.2 us
    ppermute x7, waiting for transfers between devices, per_device(): lax.ppermute(ring[-1], 'sp', [(dev, (dev + 1) % 8) for dev in range(8)])  57.2 us
    all_gather x1, waiting for transfers between devices, per_device(): wide = lax.all_gather(tokens, 'tp', axis=0, tiled=True).astype(jnp.float32)  26.9 us
    unnamed x39, local copies, waits for them, and re-layouts  13.3 us
    psum x1, blocking collectives, per_device(): lax.psum(jnp.sum(convolved * convolved, axis=1), 'tp') / all_channels  6.22 us
    reduce_sum x1, other arithmetic, per_device(): jnp.sum(convolved * convolved, axis=1)  5.58 us
  transfers between devices with their start and end apart: 11, of which 9 were waited for; matrix products, arithmetic and copies ran while one was open for 12% of the time, Pallas kernels for 0%

profile of v1, /device:TPU:0, one launch (start us, length us, event | category | flops | bytes accessed | tf_op | source)
XLA Modules:
  0.0 228.7 jit_solution(8539127337218910620)
XLA Ops:
  8.0 26.9 %all-gather.3.cloned.1.call-done = bf16[512,2048]{1,0:T(8,128)(2,1)} async-done(((bf16[128,2048]{1,0:T(8,128)(2,1)}), bf16[512,2048]{1,0:T(8,128)(2,1)}) %all-gather.3.cloned.1.call-update) | async-done | bytes 2097168 | tf_op jit(solution)/shard_map/all_gather | solution.py:33
  34.9 2.1 fusion.13
  37.0 2.6 %convolution_convert_fusion = bf16[512,256]{1,0:T(8,128)(2,1)S(1)} fusion(bf16[2048,256]{1,0:T(8,128)(2,1)} %param.20, bf16[512,2048]{1,0:T(8,128)(2,1)} %all-gather.3.cloned.1.call-done, f32[2048]{0:T(1024)} %param.17, f32[512]{0:T(512)S(1)} %add_rsqrt_fusion.1), kind=kOutput, calls=%fused_computation.34 | convolution fusion | flops 541196288 | bytes 3418112 | tf_op jit(solution)/shard_map/dot_general | solution.py:40
  39.6 1.5 collective-permute-start
  41.2 9.6 %collective-permute-done = bf16[512,256]{1,0:T(8,128)(2,1)S(1)} collective-permute-done((bf16[512,256]{1,0:T(8,128)(2,1)S(1)}, bf16[512,256]{1,0:T(8,128)(2,1)S(1)}, u32[]{:S(2)}, u32[]{:S(2)}) %collective-permute-start) | collective-permute-done | bytes 262176 | tf_op jit(solution)/shard_map/ppermute | solution.py:106
  51.5 9.6 %collective-permute-done.1 = bf16[512,256]{1,0:T(8,128)(2,1)S(1)} collective-permute-done((bf16[512,256]{1,0:T(8,128)(2,1)S(1)}, bf16[512,256]{1,0:T(8,128)(2,1)S(1)}, u32[]{:S(2)}, u32[]{:S(2)}) %collective-permute-start.1) | collective-permute-done | bytes 262176 | tf_op jit(solution)/shard_map/ppermute | solution.py:106
  61.1 3.3 %convolution_convert_fusion.1 = bf16[512,256]{1,0:T(8,128)(2,1)} fusion(bf16[2048,256]{1,0:T(8,128)(2,1)} %param.19, bf16[512,2048]{1,0:T(8,128)(2,1)} %all-gather.3.cloned.1.call-done, f32[2048]{0:T(1024)S(1)} %copy-done.8, f32[512]{0:T(512)S(1)} %add_rsqrt_fusion.1), kind=kOutput, calls=%fused_computation.35 | convolution fusion | flops 541196288 | bytes 3418112 | tf_op jit(solution)/shard_map/dot_general | solution.py:39
  64.5 6.0 %collective-permute-done.2 = bf16[512,256]{1,0:T(8,128)(2,1)S(1)} collective-permute-done((bf16[512,256]{1,0:T(8,128)(2,1)S(1)}, bf16[512,256]{1,0:T(8,128)(2,1)S(1)}, u32[]{:S(2)}, u32[]{:S(2)}) %collective-permute-start.2) | collective-permute-done | bytes 262176 | tf_op jit(solution)/shard_map/ppermute | solution.py:106
  70.5 3.8 %fusion.18 = f32[512,512]{1,0:T(8,128)S(1)} fusion(bf16[2048,512]{1,0:T(8,128)(2,1)} %param.22, bf16[512,2048]{1,0:T(8,128)(2,1)} %all-gather.3.cloned.1.call-done, f32[2048]{0:T(1024)S(1)} %copy-done.8, f32[512]{0:T(512)S(1)} %add_rsqrt_fusion.1), kind=kOutput, calls=%fused_computation.30 | convolution fusion | flops 1078722560 | bytes 5253120 | tf_op jit(solution)/shard_map/dot_general | solution.py:42
  74.3 7.1 %collective-permute-done.3 = bf16[512,256]{1,0:T(8,128)(2,1)S(1)} collective-permute-done((bf16[512,256]{1,0:T(8,128)(2,1)S(1)}, bf16[512,256]{1,0:T(8,128)(2,1)S(1)}, u32[]{:S(2)}, u32[]{:S(2)}) %collective-permute-start.3) | collective-permute-done | bytes 262176 | tf_op jit(solution)/shard_map/ppermute | solution.py:106
  84.1 9.6 %collective-permute-done.4 = bf16[512,256]{1,0:T(8,128)(2,1)S(1)} collective-permute-done((bf16[512,256]{1,0:T(8,128)(2,1)S(1)}, bf16[512,256]{1,0:T(8,128)(2,1)S(1)}, u32[]{:S(2)}, u32[]{:S(2)}) %collective-permute-start.4) | collective-permute-done | bytes 262176 | tf_op jit(solution)/shard_map/ppermute | solution.py:106
  93.6 1.6 fusion.20
  95.5 12.5 %collective-permute-done.5 = bf16[512,256]{1,0:T(8,128)(2,1)} collective-permute-done((bf16[512,256]{1,0:T(8,128)(2,1)S(1)}, bf16[512,256]{1,0:T(8,128)(2,1)}, u32[]{:S(2)}, u32[]{:S(2)}) %collective-permute-start.5) | collective-permute-done | bytes 262176 | tf_op jit(solution)/shard_map/ppermute | solution.py:106
  108.0 5.6 %multiply_reduce_fusion = (f32[512]{0:T(512)S(1)}, f32[512,512]{1,0:T(8,128)}) fusion(f32[542,512]{1,0:T(8,128)S(1)} %maximum_convert_fusion, f32[512]{0:T(512)S(1)} %bitcast.72, f32[512]{0:T(512)S(1)} %bitcast.73, f32[512]{0:T(512)S(1)} %bitcast.75, f32[512]{0:T(512)S(1)} %bitcast.76, f32[512]{0:T(512)S(1)} %bitcast.77, f32[512]{0:T(512)S(1)} %bitcast.78, ...), kind=kLoop, calls=%fused_computation.98 | loop fusion | flops 16514560 | bytes 33619968 | tf_op jit(solution)/shard_map/reduce_sum | solution.py:152
  113.6 6.2 %psum.7 = f32[512]{0:T(512)S(1)} all-reduce(f32[512]{0:T(512)S(1)} %get-tuple-element.390), channel_id=1, replica_groups=mesh['sp'=8,'tp'=4] {'tp'}, use_global_device_ids=true, to_apply=%region_8.9 | all-reduce | flops 512 | bytes 4096 | tf_op jit(solution)/shard_map/psum | solution.py:152
  119.8 2.8 %collective-permute-done.6 = bf16[512,256]{1,0:T(8,128)(2,1)} collective-permute-done((bf16[512,256]{1,0:T(8,128)(2,1)}, bf16[512,256]{1,0:T(8,128)(2,1)}, u32[]{:S(2)}, u32[]{:S(2)}) %collective-permute-start.6) | collective-permute-done | bytes 262176 | tf_op jit(solution)/shard_map/ppermute | solution.py:106
  129.3 4.2 %copy.16 = bf16[4096,256]{0,1:T(8,128)(2,1)} copy(bf16[4096,256]{1,0:T(8,128)(2,1)} %constant_dynamic-slice_fusion.3) | data formatting | bytes 4194304
  133.4 4.1 %copy.15 = bf16[4096,256]{0,1:T(8,128)(2,1)} copy(bf16[4096,256]{1,0:T(8,128)(2,1)} %all-gather.5.cloned.1.call-done) | data formatting | bytes 4194304
  137.6 6.8 %while.18 = (s32[]{:T(128)}, f32[4,512]{1,0:T(4,128)S(1)}, f32[4,512]{1,0:T(4,128)S(1)}, f32[4,512,64]{1,2,0:T(8,128)S(1)}, s32[]{:T(128)}, /*index=5*/bf16[4096...) while((s32[]{:T(128)}, f32[4,512]{1,0:T(4,128)S(1)}, ...), condition=%wide.region_6.7_spmd.clone, body=%wide.region_1.6_spmd.clone.sunk | while | flops 286005248 | bytes 16725373 | solution.py:130
  137.6 6.3 %conditional.3 = ((f32[4,512]{1,0:T(4,128)S(1)}, f32[4,512]{1,0:T(4,128)S(1)}, f32[4,512,64]{1,2,0:T(8,128)S(1)})) conditional(s32[]{:T(128)} %convert_element_type.89, (f32[4,512]{1,0:T(4,128)S(1)}, f32[4,512]{1,0:T(4,128)S(1)}, f32[4,512,64]{1,2,0:T(8,128)S(1)}) %tuple.88, (s32[]{:T(128)}, s32[]{:T(128)}, bf16[4096,256]{0,1:T(8,128)(2,1)}, ...), branch_computations={%region_2.2_spmd, %region_3.5_spmd} | conditional | flops 286005248 | bytes 16723030 | solution.py:127
  142.3 1.6 fusion.8
  144.5 2.0 fusion.63
  146.5 2.8 %add_convert_fusion = bf16[512,2048]{1,0:T(8,128)(2,1)} fusion(f32[512,2048]{1,0:T(8,128)S(1)} %fusion.63, bf16[512,2048]{1,0:T(8,128)(2,1)S(1)} %copy-done, f32[512,512]{1,0:T(8,128)S(1)} %copy-done.2, f32[512]{0:T(512)S(1)} %copy-done.9, f32[512]{0:T(512)S(1)} %add_rsqrt_fusion), kind=kOutput, calls=%fused_computation.25 | convolution fusion | flops 1077673984 | bytes 9441280 | tf_op jit(solution)/shard_map/dot_general | solution.py:157
  150.0 72.2 %reduce-scatter.2.cloned.1.call-done = bf16[128,2048]{1,0:T(8,128)(2,1)} async-done(((bf16[512,2048]{1,0:T(8,128)(2,1)}), bf16[128,2048]{1,0:T(8,128)(2,1)}) %reduce-scatter.2.cloned.1.call-update) | async-done | bytes 524304 | tf_op jit(solution)/shard_map/reduce_scatter | solution.py:158
  (92 shorter events, 16.5 us)
Async XLA Ops:
  7.2 139.3 %copy-start = (bf16[512,2048]{1,0:T(8,128)(2,1)S(1)}, bf16[512,2048]{1,0:T(8,128)(2,1)}, u32[]{:S(2)}) copy-start(bf16[512,2048]{1,0:T(8,128)(2,1)} %param.27) | copy-start | bytes 6291460
  7.2 34.0 %copy-start.5 = (f32[31,512]{1,0:T(8,128)S(1)}, f32[31,512]{1,0:T(8,128)}, u32[]{:S(2)}) copy-start(f32[31,512]{1,0:T(8,128)} %param.23) | copy-start | bytes 190468
  7.2 27.7 %all-gather.3.cloned.1.call-start = ((), (), s32[]{:S(2)}) async-start(), calls=%async_computation.1 | async-start | bytes 2621440 | tf_op jit(solution)/shard_map/all_gather | solution.py:33
  7.9 53.2 %copy-start.8 = (f32[2048]{0:T(1024)S(1)}, f32[2048]{0:T(1024)}, u32[]{:S(2)}) copy-start(f32[2048]{0:T(1024)} %param.17) | copy-start | bytes 24580
  7.9 125.5 %all-gather.5.cloned.1.call-start = ((), (), s32[]{:S(2)}) async-start(), calls=%async_computation.2 | async-start | bytes 2359296 | tf_op jit(solution)/shard_map/all_gather | solution.py:103
  39.6 11.2 %collective-permute-start = (bf16[512,256]{1,0:T(8,128)(2,1)S(1)}, bf16[512,256]{1,0:T(8,128)(2,1)S(1)}, u32[]{:S(2)}, u32[]{:S(2)}) collective-permute-start(bf16[512,256]{1,0:T(8,128)(2,1)S(1)} %convolution_convert_fusion), channel_id=1, source_target_pairs={{0,4},{4,8},{8,12},{12,16},{16,20},{20,24},{24,28},{28,0},{1,5},{5... | collective-permute-start | bytes 786440 | tf_op jit(solution)/shard_map/ppermute | solution.py:106
  50.8 10.3 %collective-permute-start.1 = (bf16[512,256]{1,0:T(8,128)(2,1)S(1)}, bf16[512,256]{1,0:T(8,128)(2,1)S(1)}, u32[]{:S(2)}, u32[]{:S(2)}) collective-permute-start(bf16[512,256]{1,0:T(8,128)(2,1)S(1)} %collective-permute-done), channel_id=1, source_target_pairs={{0,4},{4,8},{8,12},{12,16},{16,20},{20,24},{24,28},{28,0},{1,5},{5... | collective-permute-start | bytes 786440 | tf_op jit(solution)/shard_map/ppermute | solution.py:106
  61.1 9.4 %collective-permute-start.2 = (bf16[512,256]{1,0:T(8,128)(2,1)S(1)}, bf16[512,256]{1,0:T(8,128)(2,1)S(1)}, u32[]{:S(2)}, u32[]{:S(2)}) collective-permute-start(bf16[512,256]{1,0:T(8,128)(2,1)S(1)} %collective-permute-done.1), channel_id=1, source_target_pairs={{0,4},{4,8},{8,12},{12,16},{16,20},{20,24},{24,28},{28,0},{1,5},{5... | collective-permute-start | bytes 786440 | tf_op jit(solution)/shard_map/ppermute | solution.py:106
  64.4 157.8 %reduce-scatter.2.cloned.1.call-start = ((), (), s32[]{:S(2)}) async-start(), calls=%async_computation.3 | async-start | bytes 2621440 | tf_op jit(solution)/shard_map/reduce_scatter | solution.py:158
  64.5 16.9 %copy-start.1 = (bf16[512,2048]{1,0:T(8,128)(2,1)S(1)}, bf16[512,2048]{1,0:T(8,128)(2,1)}, u32[]{:S(2)}) copy-start(bf16[512,2048]{1,0:T(8,128)(2,1)} %all-gather.3.cloned.1.call-done) | copy-start | bytes 6291460
  64.5 16.9 %copy-start.6 = (bf16[2048,512]{1,0:T(8,128)(2,1)S(1)}, bf16[2048,512]{1,0:T(8,128)(2,1)}, u32[]{:S(2)}) copy-start(bf16[2048,512]{1,0:T(8,128)(2,1)} %param.21) | copy-start | bytes 6291460
  70.5 10.9 %collective-permute-start.3 = (bf16[512,256]{1,0:T(8,128)(2,1)S(1)}, bf16[512,256]{1,0:T(8,128)(2,1)S(1)}, u32[]{:S(2)}, u32[]{:S(2)}) collective-permute-start(bf16[512,256]{1,0:T(8,128)(2,1)S(1)} %collective-permute-done.2), channel_id=1, source_target_pairs={{0,4},{4,8},{8,12},{12,16},{16,20},{20,24},{24,28},{28,0},{1,5},{5... | collective-permute-start | bytes 786440 | tf_op jit(solution)/shard_map/ppermute | solution.py:106
  74.3 19.4 %copy-start.7 = (bf16[2048,256]{1,0:T(8,128)(2,1)S(1)}, bf16[2048,256]{1,0:T(8,128)(2,1)}, u32[]{:S(2)}) copy-start(bf16[2048,256]{1,0:T(8,128)(2,1)} %param.18) | copy-start | bytes 3145732
  81.4 12.2 %collective-permute-start.4 = (bf16[512,256]{1,0:T(8,128)(2,1)S(1)}, bf16[512,256]{1,0:T(8,128)(2,1)S(1)}, u32[]{:S(2)}, u32[]{:S(2)}) collective-permute-start(bf16[512,256]{1,0:T(8,128)(2,1)S(1)} %collective-permute-done.3), channel_id=1, source_target_pairs={{0,4},{4,8},{8,12},{12,16},{16,20},{20,24},{24,28},{28,0},{1,5},{5... | collective-permute-start | bytes 786440 | tf_op jit(solution)/shard_map/ppermute | solution.py:106
  82.8 12.5 %collective-permute-start.7 = (bf16[30,512]{1,0:T(8,128)(2,1)S(1)}, bf16[30,512]{1,0:T(8,128)(2,1)S(1)}, u32[]{:S(2)}, u32[]{:S(2)}) collective-permute-start(bf16[30,512]{1,0:T(8,128)(2,1)S(1)} %slice.252), channel_id=1, source_target_pairs={{0,4},{4,8},{8,12},{12,16},{16,20},{20,24},{24,28},{1,5},{5,9},{9,... | collective-permute-start | bytes 92168 | tf_op jit(solution)/shard_map/ppermute | solution.py:12
  93.6 19.9 %copy-start.3 = (bf16[512,256]{1,0:T(8,128)(2,1)}, bf16[512,256]{1,0:T(8,128)(2,1)S(1)}, u32[]{:S(2)}) copy-start(bf16[512,256]{1,0:T(8,128)(2,1)S(1)} %collective-permute-done.4) | copy-start | bytes 786436
  93.6 14.3 %collective-permute-start.5 = (bf16[512,256]{1,0:T(8,128)(2,1)S(1)}, bf16[512,256]{1,0:T(8,128)(2,1)}, u32[]{:S(2)}, u32[]{:S(2)}) collective-permute-start(bf16[512,256]{1,0:T(8,128)(2,1)S(1)} %collective-permute-done.4), channel_id=1, source_target_pairs={{0,4},{4,8},{8,12},{12,16},{16,20},{20,24},{24,28},{28,0},{1,5},{5... | collective-permute-start | bytes 786440 | tf_op jit(solution)/shard_map/ppermute | solution.py:106
  108.0 14.6 %collective-permute-start.6 = (bf16[512,256]{1,0:T(8,128)(2,1)}, bf16[512,256]{1,0:T(8,128)(2,1)}, u32[]{:S(2)}, u32[]{:S(2)}) collective-permute-start(bf16[512,256]{1,0:T(8,128)(2,1)} %collective-permute-done.5), channel_id=1, source_target_pairs={{0,4},{4,8},{8,12},{12,16},{16,20},{20,24},{24,28},{28,0},{1,5},{5... | collective-permute-start | bytes 786440 | tf_op jit(solution)/shard_map/ppermute | solution.py:106
  119.8 7.8 %copy-start.4 = (bf16[512,256]{1,0:T(8,128)(2,1)S(1)}, bf16[512,256]{1,0:T(8,128)(2,1)}, u32[]{:S(2)}) copy-start(bf16[512,256]{1,0:T(8,128)(2,1)} %copy-done.3) | copy-start | bytes 786436
  129.3 8.3 %copy-start.10 = (bf16[512,256]{0,1:T(8,128)(2,1)S(1)}, bf16[512,256]{0,1:T(8,128)(2,1)}, u32[]{:S(2)}) copy-start(bf16[512,256]{0,1:T(8,128)(2,1)} %fusion.20) | copy-start | bytes 786436
  144.4 2.1 copy-start.2
  144.4 2.1 copy-start.9
Sparse Core Ops, SparseCore 0:
  9.6 25.2 all-gather.2
  64.5 58.4 all-gather.4
  149.5 72.6 reduce-scatter.1
